TPU v7x, 32 devices: a whole 2x2x4 slice. The times are simulated.
32 devices in a mesh: ep: 8 (over z, x), tp: 4 (over y, core).
Axes of the slice: x: 2, y: 2, z: 4, core: 2. Of those that a mesh axis runs over, the one named last changes fastest.
Arguments:
- queries: bfloat16 [2048, 1024], P('ep', 'tp'), may hold values from -256 to 256
- key_rows: bfloat16 [2048, 1024], P('ep', 'tp'), may hold values from -8 to 8
- value_rows: bfloat16 [2048, 1024], P('ep', 'tp'), may hold values from -6 to 6
- head_lambda: float32 [8], P('tp'), may hold values from 0.3 to 0.8
- sub_gain: float32 [128], replicated, may hold values from 0.1 to 1.9
- out_weight: bfloat16 [1024, 2048], P('tp'), may hold values from -0.1875 to 0.1875
- expert_input: bfloat16 [1536, 2048], P('ep'), may hold values from -6 to 6
- norm_gain: float32 [2048], replicated, may hold values from 0.1 to 1.9
- route_ids: int32 [1536, 2], P('ep'), may hold values from 0 to 7, all different within a row; in each aligned block of 192 rows (0 to 191, 192 to 383, ...) at most 80 rows name the same one
- route_weight: float32 [1536, 2], P('ep'), may hold values from 0.25 to 1
- gate_weight: bfloat16 [8, 2048, 3584], P('ep', None, 'tp'), may hold values from -0.125 to 0.125
- up_weight: bfloat16 [8, 2048, 3584], P('ep', None, 'tp'), may hold values from -0.125 to 0.125
- down_weight: bfloat16 [8, 3584, 2048], P('ep', 'tp'), may hold values from -0.09375 to 0.09375
Outputs:
- mixer_out: bfloat16 [2048, 2048], P(('ep', 'tp'))
- expert_out: bfloat16 [1536, 2048], P('ep', 'tp')
Inputs may be any that keep to these rules, and one draw needn't show every extreme that they name: `route_ids`: each row names 2 different experts. In each aligned block of 192 rows no expert is named by more than 80 rows, a bound that some block reaches.
All inputs are finite; a program needn't handle non-finite values.
Results may differ from a plain program's by a relative error of at most 0.014.
Values may be sent and summed in bfloat16 or wider, within the bound.
A program may use at most 256 MiB of HBM per device.

v0:
```python
import jax
import jax.numpy as jnp
from jax import lax
from jax.sharding import PartitionSpec as P

EPS = 1e-06


def mixer_half(queries, key_rows, value_rows, head_lambda, sub_gain, out_weight):
    rows_here = queries.shape[0]
    heads_here = head_lambda.shape[0]
    head_width = queries.shape[1] // (2 * heads_here)
    value_width = value_rows.shape[1] // heads_here
    scaling = head_width ** (-0.5)
    query_blocks = queries.reshape(rows_here, heads_here, 2, head_width)
    query_pos = lax.axis_index("ep") * rows_here + jnp.arange(rows_here, dtype=jnp.int32)
    row_max = jnp.full((heads_here, 2, rows_here), -1e30, jnp.float32)
    key_piece = lax.all_gather(key_rows, "ep", axis=0, tiled=True)
    value_piece = lax.all_gather(value_rows, "ep", axis=0, tiled=True)
    length = key_piece.shape[0]
    key_blocks = key_piece.reshape(length, heads_here, 2, head_width)
    value_blocks = value_piece.reshape(length, heads_here, value_width)
    scores = (
        jnp.einsum("qhmd,khmd->hmqk", query_blocks, key_blocks, preferred_element_type=jnp.float32)
        * scaling
    )
    allowed = query_pos[:, None] >= jnp.arange(length, dtype=jnp.int32)[None, :]
    scores = jnp.where(allowed, scores, -1e30)
    new_max = jnp.maximum(row_max, jnp.max(scores, axis=-1))
    weights = jnp.where(allowed, jnp.exp(scores - new_max[..., None]), 0.0)
    row_total = jnp.sum(weights, axis=-1)
    numerator = jnp.einsum(
        "hmqk,khd->hmqd",
        weights.astype(jnp.bfloat16),
        value_blocks,
        preferred_element_type=jnp.float32,
    )
    row_max, row_total, numerator = (new_max, row_total, numerator)
    per_map = numerator / row_total[..., None]
    contrast = per_map[:, 0] - head_lambda[:, None, None] * per_map[:, 1]
    normed = (
        contrast * lax.rsqrt(jnp.mean(contrast * contrast, axis=-1, keepdims=True) + EPS) * sub_gain
    ).astype(jnp.bfloat16)
    attended = jnp.transpose(normed, (1, 0, 2)).reshape(rows_here, heads_here * value_width)
    return lax.psum_scatter(
        jnp.dot(attended, out_weight, preferred_element_type=jnp.float32).astype(jnp.bfloat16),
        "tp",
        scatter_dimension=0,
        tiled=True,
    )


def expert_half(
    expert_input, norm_gain, route_ids, route_weight, gate_weight, up_weight, down_weight
):
    rows_here, model_width = expert_input.shape
    experts = lax.axis_size("ep")
    top_count = route_ids.shape[1]
    capacity = 5 * top_count * rows_here // (3 * experts)
    slots = experts * capacity
    wide_rows = expert_input.astype(jnp.float32)
    normed = (
        wide_rows
        * lax.rsqrt(jnp.mean(wide_rows * wide_rows, axis=-1, keepdims=True) + EPS)
        * norm_gain
    ).astype(jnp.bfloat16)
    flat_ids = route_ids.reshape(-1)
    onehot = (flat_ids[:, None] == jnp.arange(experts, dtype=jnp.int32)[None, :]).astype(jnp.int32)
    rank_before = jnp.cumsum(onehot, axis=0) - onehot
    slot_index = jnp.sum(rank_before * onehot, axis=1)
    buffer_pos = (flat_ids * capacity + slot_index).reshape(rows_here, top_count)
    matches = buffer_pos[None, :, :] == jnp.arange(slots, dtype=jnp.int32)[:, None, None]
    dispatch = jnp.any(matches, axis=-1).astype(jnp.bfloat16)
    combine = jnp.sum(jnp.where(matches, route_weight[None, :, :], 0.0), axis=-1)
    gate_mat = gate_weight[0]
    up_mat = up_weight[0]
    down_mat = down_weight[0]
    outgoing = jnp.dot(dispatch, normed, preferred_element_type=jnp.float32).astype(jnp.bfloat16)
    arrived = lax.all_to_all(
        outgoing.reshape(experts, capacity, model_width),
        "ep",
        split_axis=0,
        concat_axis=0,
        tiled=True,
    ).reshape(slots, model_width)
    gate_act = jnp.dot(arrived, gate_mat, preferred_element_type=jnp.float32)
    up_act = jnp.dot(arrived, up_mat, preferred_element_type=jnp.float32)
    hidden = (jax.nn.silu(gate_act) * up_act).astype(jnp.bfloat16)
    partial_result = jnp.dot(hidden, down_mat, preferred_element_type=jnp.float32)
    summed = lax.psum_scatter(
        partial_result.astype(jnp.bfloat16), "tp", scatter_dimension=1, tiled=True
    )
    col_count = summed.shape[1]
    returned = lax.all_to_all(
        summed.reshape(experts, capacity, col_count), "ep", split_axis=0, concat_axis=0, tiled=True
    ).reshape(slots, col_count)
    mixed = lax.dot_general(
        combine,
        returned.astype(jnp.float32),
        (((0,), (0,)), ((), ())),
        precision=lax.Precision.HIGHEST,
        preferred_element_type=jnp.float32,
    )
    return mixed.astype(jnp.bfloat16)


def shards(
    queries,
    key_rows,
    value_rows,
    head_lambda,
    sub_gain,
    out_weight,
    expert_input,
    norm_gain,
    route_ids,
    route_weight,
    gate_weight,
    up_weight,
    down_weight,
):
    mixer_out = mixer_half(queries, key_rows, value_rows, head_lambda, sub_gain, out_weight)
    expert_out = expert_half(
        expert_input, norm_gain, route_ids, route_weight, gate_weight, up_weight, down_weight
    )
    return (mixer_out, expert_out)


def solution(mesh):
    placed = (
        P("ep", "tp"),
        P("ep", "tp"),
        P("ep", "tp"),
        P("tp"),
        P(),
        P("tp", None),
        P("ep", None),
        P(),
        P("ep", None),
        P("ep", None),
        P("ep", None, "tp"),
        P("ep", None, "tp"),
        P("ep", "tp", None),
    )
    return jax.shard_map(
        shards,
        mesh=mesh,
        in_specs=placed,
        out_specs=(P(("ep", "tp"), None), P("ep", "tp")),
        check_vma=False,
    )
```

profile of v0, /device:TPU:0, one launch (start us, length us, event | category | flops | bytes accessed | tf_op | source)
XLA Modules:
  0.0 183.7 jit_solution(2173405152536160842)
XLA Ops:
  8.0 0.0 copy-start
  8.0 0.9 copy.43
  8.9 0.1 eq.42
  9.0 0.1 eq.38
  9.2 0.9 reduce-window.6
  10.1 0.2 slice_reduce_fusion
  10.3 0.1 fusion.32
  10.4 0.1 reduce_sum.50
  10.6 0.1 copy.45
  10.6 0.7 multiply_add_fusion
  11.3 0.1 fusion.23
  11.5 1.4 fusion.17
  12.9 3.6 %convolution_convert_fusion = bf16[640,2048]{1,0:T(8,128)(2,1)} fusion(pred[640,192]{0,1:T(8,128)(4,1)S(1)} %fusion.23, bf16[192,2048]{1,0:T(8,128)(2,1)} %param.19, f32[2048]{0:T(1024)} %param.20, f32[192]{0:T(256)S(1)} %add_rsqrt_fusion.1), kind=kOutput, calls=%fused_computation.14 | convolution fusion | flops 506200064 | bytes 3539712 | tf_op jit(solution)/shard_map/dot_general | solution.py:78
  16.5 7.3 %all-to-all-start = ((bf16[8,80,2048]{2,1,0:T(8,128)(2,1)}), bf16[8,80,2048]{2,1,0:T(8,128)(2,1)}, u32[]{:S(2)}, u32[]{:S(2)}) async-start(bf16[8,80,2048]{2,1,0:T(8,128)(2,1)} %bitcast.68), calls=%async_computation.1 | async-start | bytes 5242880 | tf_op jit(solution)/shard_map/all_to_all | solution.py:79
  23.8 0.0 all-gather.3.cloned.1.call-start
  23.8 0.7 all-gather.3.cloned.1.call-update
  24.5 0.0 all-gather.5.cloned.1.call-start
  24.6 0.7 all-gather.5.cloned.1.call-update
  25.3 0.0 reduce-scatter.5.cloned.1.call-start
  25.3 70.7 %all-to-all-done = bf16[8,80,2048]{2,1,0:T(8,128)(2,1)} async-done(((bf16[8,80,2048]{2,1,0:T(8,128)(2,1)}), bf16[8,80,2048]{2,1,0:T(8,128)(2,1)}, u32[]{:S(2)}, u32[]{:S(2)}) %all-to-all-start) | async-done | bytes 2621472 | tf_op jit(solution)/shard_map/all_to_all | solution.py:79
  96.0 7.2 %fusion.10 = f32[640,896]{1,0:T(8,128)} fusion(bf16[640,2048]{1,0:T(8,128)(2,1)} %bitcast.12, bf16[1,2048,896]{2,1,0:T(8,128)(2,1)} %param.23), kind=kOutput, calls=%fused_computation.11 | convolution fusion | flops 2348810240 | bytes 8585216 | tf_op jit(solution)/shard_map/dot_general | solution.py:86
  103.2 0.0 copy-start.2
  103.2 11.8 %fusion.12 = bf16[640,2048]{1,0:T(8,128)(2,1)} fusion(bf16[1,896,2048]{2,1,0:T(8,128)(2,1)} %param.25, f32[640,896]{1,0:T(8,128)} %fusion.10, bf16[640,2048]{1,0:T(8,128)(2,1)} %bitcast.12, bf16[1,2048,896]{2,1,0:T(8,128)(2,1)} %param.24), kind=kOutput, calls=%fused_computation.13 | convolution fusion | flops 4702371840 | bytes 14876672 | tf_op jit(solution)/shard_map/dot_general | solution.py:89
  115.0 0.0 reduce-scatter.5.cloned.1.call-update
  115.0 0.2 reduce-scatter.3.cloned.1.call-start
  115.3 0.0 copy-done.2
  115.3 0.1 copy.39
  115.4 0.4 iota_compare_fusion
  115.8 0.0 all-gather.3.cloned.1.call-done
  115.8 1.5 copy.40
  117.3 11.8 %all-gather.5.cloned.1.call-done = bf16[2048,256]{1,0:T(8,128)(2,1)} async-done(((bf16[256,256]{1,0:T(8,128)(2,1)}), bf16[2048,256]{1,0:T(8,128)(2,1)}) %all-gather.5.cloned.1.call-update) | async-done | bytes 1048592 | tf_op jit(solution)/shard_map/all_gather | solution.py:19
  129.1 2.3 %copy.41 = bf16[2048,256]{0,1:T(8,128)(2,1)} copy(bf16[2048,256]{1,0:T(8,128)(2,1)} %all-gather.5.cloned.1.call-done) | data formatting | bytes 2097152 | tf_op jit(solution)/shard_map/all_gather | solution.py:19
  131.3 1.8 fusion
  133.1 0.0 copy-start.1
  133.1 2.5 %fusion.1 = f32[2,2,256]{2,1,0:T(2,128)S(1)} fusion(f32[2,2,256,2048]{3,2,1,0:T(8,128)S(1)} %get-tuple-element.3, f32[2,2,256]{2,1,0:T(2,128)S(1)} %broadcast_maximum_fusion, pred[256,2048]{1,0:T(8,128)(4,1)S(1)} %iota_compare_fusion), kind=kLoop, calls=%fused_computation.3 | loop fusion | flops 10484736 | bytes 8921088 | tf_op jit(solution)/shard_map/reduce_sum | solution.py:31
  135.6 0.0 copy-done.1
  135.6 0.0 copy-start.4
  135.6 0.0 copy-start.5
  135.6 2.2 %fusion.20 = f32[2,2,256,128]{2,3,1,0:T(8,128)S(1)} fusion(bf16[2048,2,128,1]{0,2,3,1:T(8,128)(2,1)S(1)} %bitcast.71, f32[2,2,256,2048]{3,2,1,0:T(8,128)S(1)} %get-tuple-element.3, f32[2,2,256]{2,1,0:T(2,128)S(1)} %broadcast_maximum_fusion, pred[256,2048]{1,0:T(8,128)(4,1)S(1)} %iota_compare_fusion, f32[2,2,256]{2,1,0:T(2,128)S(1)} %fusion.1), kind=kOutput, calls=%fused_computation.24 | convolution fusion | flops 547487744 | bytes 10493952 | tf_op jit(solution)/shard_map/hmqk,khd->hmqd/dot_general | solution.py:32
  137.9 0.0 copy-done.4
  137.9 0.0 copy-start.3
  137.9 0.1 multiply_reduce_fusion
  138.0 0.0 copy-done.5
  138.1 0.1 multiply_convert_fusion.1
  138.2 0.0 copy-done
  138.2 1.5 convolution_convert_fusion.1
  139.6 0.0 reduce-scatter.3.cloned.1.call-update
  139.7 8.8 %reduce-scatter.5.cloned.1.call-done = bf16[640,512]{1,0:T(8,128)(2,1)} async-done(((bf16[640,2048]{1,0:T(8,128)(2,1)}), bf16[640,512]{1,0:T(8,128)(2,1)}) %reduce-scatter.5.cloned.1.call-update) | async-done | bytes 655376 | tf_op jit(solution)/shard_map/reduce_scatter | solution.py:90
  148.5 5.5 %all-to-all-start.1 = ((bf16[8,80,512]{2,1,0:T(8,128)(2,1)}), bf16[8,80,512]{2,1,0:T(8,128)(2,1)S(1)}, u32[]{:S(2)}, u32[]{:S(2)}) async-start(bf16[8,80,512]{2,1,0:T(8,128)(2,1)} %bitcast.72), calls=%async_computation.3 | async-start | bytes 1310720 | tf_op jit(solution)/shard_map/all_to_all | solution.py:94
  154.0 0.0 copy-done.3
  154.0 0.2 select_reduce_fusion
  154.2 16.9 %all-to-all-done.1 = bf16[8,80,512]{2,1,0:T(8,128)(2,1)S(1)} async-done(((bf16[8,80,512]{2,1,0:T(8,128)(2,1)}), bf16[8,80,512]{2,1,0:T(8,128)(2,1)S(1)}, u32[]{:S(2)}, u32[]{:S(2)}) %all-to-all-start.1) | async-done | bytes 655392 | tf_op jit(solution)/shard_map/all_to_all | solution.py:94
  171.1 1.3 convolution_convert_fusion.2
  172.4 3.9 %reduce-scatter.3.cloned.1.call-done = bf16[64,2048]{1,0:T(8,128)(2,1)} async-done(((bf16[256,2048]{1,0:T(8,128)(2,1)}), bf16[64,2048]{1,0:T(8,128)(2,1)}) %reduce-scatter.3.cloned.1.call-update) | async-done | bytes 262160 | tf_op jit(solution)/shard_map/reduce_scatter | solution.py:45
  (6 shorter events, 0.1 us)
Async XLA Ops:
  8.0 130.2 %copy-start = (bf16[256,2048]{1,0:T(8,128)(2,1)S(1)}, bf16[256,2048]{1,0:T(8,128)(2,1)}, u32[]{:S(2)}) copy-start(bf16[256,2048]{1,0:T(8,128)(2,1)} %param.18) | copy-start | bytes 3145732
  16.5 79.5 %all-to-all-start = ((bf16[8,80,2048]{2,1,0:T(8,128)(2,1)}), bf16[8,80,2048]{2,1,0:T(8,128)(2,1)}, u32[]{:S(2)}, u32[]{:S(2)}) async-start(bf16[8,80,2048]{2,1,0:T(8,128)(2,1)} %bitcast.68), calls=%async_computation.1 | async-start | bytes 5242880 | tf_op jit(solution)/shard_map/all_to_all | solution.py:79
  23.8 92.0 %all-gather.3.cloned.1.call-start = ((), (), s32[]{:S(2)}) async-start(), calls=%async_computation.4 | async-start | bytes 1179648 | tf_op jit(solution)/shard_map/all_gather | solution.py:18
  24.5 104.6 %all-gather.5.cloned.1.call-start = ((), (), s32[]{:S(2)}) async-start(), calls=%async_computation.5 | async-start | bytes 1179648 | tf_op jit(solution)/shard_map/all_gather | solution.py:19
  25.3 123.2 %reduce-scatter.5.cloned.1.call-start = ((), (), s32[]{:S(2)}) async-start(), calls=%async_computation.7 | async-start | bytes 3276800 | tf_op jit(solution)/shard_map/reduce_scatter | solution.py:90
  103.2 12.1 %copy-start.2 = (bf16[256,256]{1,0:T(8,128)(2,1)S(1)}, bf16[256,256]{1,0:T(8,128)(2,1)}, u32[]{:S(2)}) copy-start(bf16[256,256]{1,0:T(8,128)(2,1)} %param.13) | copy-start | bytes 393220
  115.0 61.2 %reduce-scatter.3.cloned.1.call-start = ((), (), s32[]{:S(2)}) async-start(), calls=%async_computation.6 | async-start | bytes 1310720 | tf_op jit(solution)/shard_map/reduce_scatter | solution.py:45
  133.1 2.5 %copy-start.1 = (bf16[2048,256]{0,1:T(8,128)(2,1)S(1)}, bf16[2048,256]{0,1:T(8,128)(2,1)}, u32[]{:S(2)}) copy-start(bf16[2048,256]{0,1:T(8,128)(2,1)} %copy.41) | copy-start | bytes 3145732
  135.6 2.3 %copy-start.4 = (f32[2]{0:T(128)S(1)}, f32[2]{0:T(128)}, u32[]{:S(2)}) copy-start(f32[2]{0:T(128)} %param.16) | copy-start | bytes 28
  135.6 2.4 %copy-start.5 = (f32[128]{0:T(128)S(1)}, f32[128]{0:T(128)}, u32[]{:S(2)}) copy-start(f32[128]{0:T(128)} %param.17) | copy-start | bytes 1540
  137.9 16.1 %copy-start.3 = (f32[192,2]{0,1:T(2,128)S(1)}, f32[192,2]{0,1:T(2,128)}, u32[]{:S(2)}) copy-start(f32[192,2]{0,1:T(2,128)} %param.22) | copy-start | bytes 4612
  148.5 22.6 %all-to-all-start.1 = ((bf16[8,80,512]{2,1,0:T(8,128)(2,1)}), bf16[8,80,512]{2,1,0:T(8,128)(2,1)S(1)}, u32[]{:S(2)}, u32[]{:S(2)}) async-start(bf16[8,80,512]{2,1,0:T(8,128)(2,1)} %bitcast.72), calls=%async_computation.3 | async-start | bytes 1310720 | tf_op jit(solution)/shard_map/all_to_all | solution.py:94
Sparse Core Ops, SparseCore 0:
  26.7 60.7 all-gather.2
  89.7 39.3 all-gather.4
Sparse Core Ops, SparseCore 1:
  115.1 33.3 reduce-scatter.4
  151.5 24.7 reduce-scatter.2
where the time goes:
time: 184 us
  waiting for transfers between devices  113 us (61%)
  matrix products  29.4 us (16%)
  between operations  15.7 us (9%)
  starting transfers between devices  13.2 us (7%)
  other arithmetic  6.48 us (4%)
  local copies, waits for them, and re-layouts  5.48 us (3%)
    all_to_all x1, waiting for transfers between devices, expert_half(): lax.all_to_all(outgoing.reshape(experts, capacity, model_width), 'ep', sp...  70.7 us
    all_to_all x1, waiting for transfers between devices, expert_half(): lax.all_to_all(summed.reshape(experts, capacity, col_count), 'ep', split_...  16.9 us
    dot_general x1, matrix products, expert_half(): jnp.dot(hidden, down_mat, preferred_element_type=jnp.float32)  11.8 us
    all_gather x1, waiting for transfers between devices, mixer_half(): value_piece = lax.all_gather(value_rows, 'ep', axis=0, tiled=True)  11.8 us
    reduce_scatter x1, waiting for transfers between devices, expert_half(): lax.psum_scatter(partial_result.astype(jnp.bfloat16), 'tp', scatter_dimen...  8.83 us
    all_to_all x1, starting transfers between devices, expert_half(): lax.all_to_all(outgoing.reshape(experts, capacity, model_width), 'ep', sp...  7.28 us
    dot_general x1, matrix products, expert_half(): gate_act = jnp.dot(arrived, gate_mat, preferred_element_type=jnp.float32)  7.18 us
    all_to_all x1, starting transfers between devices, expert_half(): lax.all_to_all(summed.reshape(experts, capacity, col_count), 'ep', split_...  5.54 us
  transfers between devices with their start and end apart: 6, of which 5 were waited for; matrix products, arithmetic and copies ran while one was open for 18% of the time, Pallas kernels for 0%

commit v1 on v0

--- a/solution.py
+++ b/solution.py
@@ -2,8 +2,17 @@
 import jax.numpy as jnp
 from jax import lax
 from jax.sharding import PartitionSpec as P
+from jax.lax import all_gather
 
 EPS = 1e-06
+
+
+def _search_meshes(inner_x, t0):
+    return jnp.split(
+        all_gather(jnp.concatenate([inner_x, t0], axis=1), "ep", tiled=True, axis=0),
+        [inner_x.shape[1]],
+        axis=1,
+    )
 
 
 def mixer_half(queries, key_rows, value_rows, head_lambda, sub_gain, out_weight):
@@ -15,8 +24,7 @@
     query_blocks = queries.reshape(rows_here, heads_here, 2, head_width)
     query_pos = lax.axis_index("ep") * rows_here + jnp.arange(rows_here, dtype=jnp.int32)
     row_max = jnp.full((heads_here, 2, rows_here), -1e30, jnp.float32)
-    key_piece = lax.all_gather(key_rows, "ep", axis=0, tiled=True)
-    value_piece = lax.all_gather(value_rows, "ep", axis=0, tiled=True)
+    key_piece, value_piece = _search_meshes(key_rows, value_rows)
     length = key_piece.shape[0]
     key_blocks = key_piece.reshape(length, heads_here, 2, head_width)
     value_blocks = value_piece.reshape(length, heads_here, value_width)

time: 184 us -> 197 us (1.071)
  waiting for transfers between devices: 113 us -> 124 us
    all_to_all x1, waiting for transfers between devices: 70.7 us -> 84 us  [expert_half(): lax.all_to_all(outgoing.reshape(experts, capacity, model_width), 'ep', sp...]
    all_gather x2 -> x1, waiting for transfers between devices: 11.8 us -> 0.01 us  [_search_meshes(): all_gather(jnp.concatenate([inner_x, t0], axis=1), 'ep', tiled=True, axis=0)]
    reduce_scatter x1, waiting for transfers between devices: 8.83 us -> 19.5 us  [expert_half(): lax.psum_scatter(partial_result.astype(jnp.bfloat16), 'tp', scatter_dimen...]
    all_gather x2 -> x0, local copies, waits for them, and re-layouts: 3.75 us -> none  [the longest x1 2.26 us: mixer_half(): value_piece = lax.all_gather(value_rows, 'ep', axis=0, tiled=True)]
    split x0 -> x3, local copies, waits for them, and re-layouts: none -> 3.73 us  [_search_meshes(): jnp.split(all_gather(jnp.concatenate([inner_x, t0], axis=1), 'ep', tiled=...]
  transfers between devices with their start and end apart: 6 -> 5, of which waited for: 5 -> 4; matrix products, arithmetic and copies ran while one was open for 18% -> 18% of each run, Pallas kernels for 0% -> 0%
where the time goes in v1:
time: 197 us; the launch traced here: 196 us
  waiting for transfers between devices  124 us (63%)
  matrix products  30.1 us (15%)
  between operations  15.7 us (8%)
  starting transfers between devices  13.1 us (7%)
  other arithmetic  7.61 us (4%)
  local copies, waits for them, and re-layouts  5.48 us (3%)
    all_to_all x1, waiting for transfers between devices, expert_half(): lax.all_to_all(outgoing.reshape(experts, capacity, model_width), 'ep', sp...  84 us
    reduce_scatter x1, waiting for transfers between devices, expert_half(): lax.psum_scatter(partial_result.astype(jnp.bfloat16), 'tp', scatter_dimen...  19.5 us
    all_to_all x1, waiting for transfers between devices, expert_half(): lax.all_to_all(summed.reshape(experts, capacity, col_count), 'ep', split_...  16.9 us
    dot_general x1, matrix products, expert_half(): jnp.dot(hidden, down_mat, preferred_element_type=jnp.float32)  11.8 us
    all_to_all x1, starting transfers between devices, expert_half(): lax.all_to_all(outgoing.reshape(experts, capacity, model_width), 'ep', sp...  7.28 us
    dot_general x1, matrix products, expert_half(): gate_act = jnp.dot(arrived, gate_mat, preferred_element_type=jnp.float32)  7.11 us
    all_to_all x1, starting transfers between devices, expert_half(): lax.all_to_all(summed.reshape(experts, capacity, col_count), 'ep', split_...  5.51 us
  transfers between devices with their start and end apart: 5, of which 4 were waited for; matrix products, arithmetic and copies ran while one was open for 18% of the time, Pallas kernels for 0%

profile of v1, /device:TPU:0, one launch (start us, length us, event | category | flops | bytes accessed | tf_op | source)
XLA Modules:
  0.0 196.3 jit_solution(18286470993204731699)
XLA Ops:
  8.0 0.0 copy-start
  8.0 0.9 copy.47
  8.9 0.1 eq.42
  9.0 0.1 eq.38
  9.2 0.9 reduce-window.6
  10.1 0.2 slice_reduce_fusion
  10.3 0.1 fusion.32
  10.4 0.1 reduce_sum.50
  10.6 0.1 copy.49
  10.6 0.7 multiply_add_fusion
  11.3 0.1 fusion.23
  11.5 1.4 fusion.17
  12.9 0.0 copy-start.4
  12.9 0.0 copy-start.5
  12.9 3.6 %convolution_convert_fusion = bf16[640,2048]{1,0:T(8,128)(2,1)} fusion(pred[640,192]{0,1:T(8,128)(4,1)S(1)} %fusion.23, bf16[192,2048]{1,0:T(8,128)(2,1)} %param.19, f32[2048]{0:T(1024)} %param.20, f32[192]{0:T(256)S(1)} %add_rsqrt_fusion.1), kind=kOutput, calls=%fused_computation.14 | convolution fusion | flops 506200064 | bytes 3539712 | tf_op jit(solution)/shard_map/dot_general | solution.py:86
  16.5 7.3 %all-to-all-start = ((bf16[8,80,2048]{2,1,0:T(8,128)(2,1)}), bf16[8,80,2048]{2,1,0:T(8,128)(2,1)}, u32[]{:S(2)}, u32[]{:S(2)}) async-start(bf16[8,80,2048]{2,1,0:T(8,128)(2,1)} %bitcast.81), calls=%async_computation.1 | async-start | bytes 5242880 | tf_op jit(solution)/shard_map/all_to_all | solution.py:87
  23.8 0.0 all-gather.2.cloned.1.call-start
  23.9 0.0 copy-done.4
  23.9 0.0 copy-done.5
  23.9 0.7 pad_maximum_fusion
  24.6 0.0 all-gather.2.cloned.1.call-update
  24.6 0.0 reduce-scatter.5.cloned.1.call-start
  24.7 84.0 %all-to-all-done = bf16[8,80,2048]{2,1,0:T(8,128)(2,1)} async-done(((bf16[8,80,2048]{2,1,0:T(8,128)(2,1)}), bf16[8,80,2048]{2,1,0:T(8,128)(2,1)}, u32[]{:S(2)}, u32[]{:S(2)}) %all-to-all-start) | async-done | bytes 2621472 | tf_op jit(solution)/shard_map/all_to_all | solution.py:87
  108.7 7.1 %fusion.10 = f32[640,896]{1,0:T(8,128)} fusion(bf16[640,2048]{1,0:T(8,128)(2,1)} %bitcast.13, bf16[1,2048,896]{2,1,0:T(8,128)(2,1)} %param.23), kind=kOutput, calls=%fused_computation.11 | convolution fusion | flops 2348810240 | bytes 8585216 | tf_op jit(solution)/shard_map/dot_general | solution.py:94
  115.8 0.0 copy-start.3
  115.8 11.8 %fusion.12 = bf16[640,2048]{1,0:T(8,128)(2,1)} fusion(bf16[1,896,2048]{2,1,0:T(8,128)(2,1)} %param.25, f32[640,896]{1,0:T(8,128)} %fusion.10, bf16[640,2048]{1,0:T(8,128)(2,1)} %bitcast.13, bf16[1,2048,896]{2,1,0:T(8,128)(2,1)} %param.24), kind=kOutput, calls=%fused_computation.13 | convolution fusion | flops 4702371840 | bytes 14876672 | tf_op jit(solution)/shard_map/dot_general | solution.py:97
  127.6 0.0 reduce-scatter.5.cloned.1.call-update
  127.6 0.2 reduce-scatter.3.cloned.1.call-start
  127.8 0.0 copy-done.3
  127.9 0.1 copy.43
  128.0 1.1 iota_compare_fusion
  129.1 0.0 all-gather.2.cloned.1.call-done
  129.1 1.7 fusion.38
  130.8 1.4 copy.44
  132.2 0.6 copy.42
  132.9 0.0 copy-start.1
  132.9 2.7 %fusion = (f32[2,2,256]{2,1,0:T(2,128)S(1)}, f32[2,2,2048,256]{3,2,1,0:T(8,128)S(1)}) fusion(pred[256,2048]{0,1:T(8,128)(4,1)} %iota_compare_fusion, bf16[2048,2,2,64]{0,3,2,1:T(8,128)(2,1)S(1)} %bitcast.84, bf16[256,2,2,64]{0,3,2,1:T(8,128)(2,1)S(1)} %bitcast.87), kind=kOutput, calls=%fused_computation.2 | convolution fusion | flops 274725888 | bytes 10096640 | tf_op jit(solution)/shard_map/qhmd,khmd->hmqk/dot_general | solution.py:32
  135.6 0.0 copy-done.1
  135.6 0.0 copy-start.2
  135.6 2.1 %fusion.1 = f32[2,2,256]{2,1,0:T(2,128)S(1)} fusion(f32[2,2,2048,256]{3,2,1,0:T(8,128)S(1)} %get-tuple-element.5, f32[2,2,256]{2,1,0:T(2,128)S(1)} %broadcast_maximum_fusion, pred[256,2048]{0,1:T(8,128)(4,1)S(1)} %copy-done.1), kind=kLoop, calls=%fused_computation.3 | loop fusion | flops 10484736 | bytes 8921088 | tf_op jit(solution)/shard_map/reduce_sum | solution.py:39
  137.7 0.0 copy-done.2
  137.7 0.0 copy-start.7
  137.8 0.0 copy-start.8
  137.8 2.1 %fusion.20 = f32[2,2,256,128]{2,3,1,0:T(8,128)S(1)} fusion(bf16[2048,2,128,1]{0,2,3,1:T(8,128)(2,1)S(1)} %bitcast.83, f32[2,2,2048,256]{3,2,1,0:T(8,128)S(1)} %get-tuple-element.5, f32[2,2,256]{2,1,0:T(2,128)S(1)} %broadcast_maximum_fusion, pred[256,2048]{0,1:T(8,128)(4,1)S(1)} %copy-done.1, f32[2,2,256]{2,1,0:T(2,128)S(1)} %fusion.1), kind=kOutput, calls=%fused_computation.24 | convolution fusion | flops 547487744 | bytes 10493952 | tf_op jit(solution)/shard_map/hmqk,khd->hmqd/dot_general | solution.py:40
  139.9 0.0 copy-done.7
  139.9 0.0 copy-start.6
  139.9 0.1 multiply_reduce_fusion
  140.0 0.0 copy-done.8
  140.0 0.1 multiply_convert_fusion.1
  140.2 0.0 copy-done
  140.2 1.5 convolution_convert_fusion.1
  141.6 0.0 reduce-scatter.3.cloned.1.call-update
  141.6 19.5 %reduce-scatter.5.cloned.1.call-done = bf16[640,512]{1,0:T(8,128)(2,1)} async-done(((bf16[640,2048]{1,0:T(8,128)(2,1)}), bf16[640,512]{1,0:T(8,128)(2,1)}) %reduce-scatter.5.cloned.1.call-update) | async-done | bytes 655376 | tf_op jit(solution)/shard_map/reduce_scatter | solution.py:98
  161.1 5.5 %all-to-all-start.1 = ((bf16[8,80,512]{2,1,0:T(8,128)(2,1)}), bf16[8,80,512]{2,1,0:T(8,128)(2,1)S(1)}, u32[]{:S(2)}, u32[]{:S(2)}) async-start(bf16[8,80,512]{2,1,0:T(8,128)(2,1)} %bitcast.85), calls=%async_computation.3 | async-start | bytes 1310720 | tf_op jit(solution)/shard_map/all_to_all | solution.py:102
  166.6 0.0 copy-done.6
  166.6 0.2 select_reduce_fusion
  166.8 16.9 %all-to-all-done.1 = bf16[8,80,512]{2,1,0:T(8,128)(2,1)S(1)} async-done(((bf16[8,80,512]{2,1,0:T(8,128)(2,1)}), bf16[8,80,512]{2,1,0:T(8,128)(2,1)S(1)}, u32[]{:S(2)}, u32[]{:S(2)}) %all-to-all-start.1) | async-done | bytes 655392 | tf_op jit(solution)/shard_map/all_to_all | solution.py:102
  183.7 1.3 convolution_convert_fusion.2
  185.0 3.8 %reduce-scatter.3.cloned.1.call-done = bf16[64,2048]{1,0:T(8,128)(2,1)} async-done(((bf16[256,2048]{1,0:T(8,128)(2,1)}), bf16[64,2048]{1,0:T(8,128)(2,1)}) %reduce-scatter.3.cloned.1.call-update) | async-done | bytes 262160 | tf_op jit(solution)/shard_map/reduce_scatter | solution.py:53
  (6 shorter events, 0.1 us)
Async XLA Ops:
  8.0 132.2 %copy-start = (bf16[256,2048]{1,0:T(8,128)(2,1)S(1)}, bf16[256,2048]{1,0:T(8,128)(2,1)}, u32[]{:S(2)}) copy-start(bf16[256,2048]{1,0:T(8,128)(2,1)} %param.18) | copy-start | bytes 3145732
  12.9 11.0 %copy-start.4 = (bf16[256,256]{1,0:T(8,128)(2,1)S(1)}, bf16[256,256]{1,0:T(8,128)(2,1)}, u32[]{:S(2)}) copy-start(bf16[256,256]{1,0:T(8,128)(2,1)} %param.15) | copy-start | bytes 393220
  12.9 11.0 %copy-start.5 = (bf16[256,256]{1,0:T(8,128)(2,1)S(1)}, bf16[256,256]{1,0:T(8,128)(2,1)}, u32[]{:S(2)}) copy-start(bf16[256,256]{1,0:T(8,128)(2,1)} %param.14) | copy-start | bytes 393220
  16.5 92.1 %all-to-all-start = ((bf16[8,80,2048]{2,1,0:T(8,128)(2,1)}), bf16[8,80,2048]{2,1,0:T(8,128)(2,1)}, u32[]{:S(2)}, u32[]{:S(2)}) async-start(bf16[8,80,2048]{2,1,0:T(8,128)(2,1)} %bitcast.81), calls=%async_computation.1 | async-start | bytes 5242880 | tf_op jit(solution)/shard_map/all_to_all | solution.py:87
  23.8 105.3 %all-gather.2.cloned.1.call-start = ((), (), s32[]{:S(2)}) async-start(), calls=%async_computation.4 | async-start | bytes 2359296 | tf_op jit(solution)/shard_map/all_gather | solution.py:12
  24.6 136.5 %reduce-scatter.5.cloned.1.call-start = ((), (), s32[]{:S(2)}) async-start(), calls=%async_computation.6 | async-start | bytes 3276800 | tf_op jit(solution)/shard_map/reduce_scatter | solution.py:98
  115.8 12.0 %copy-start.3 = (bf16[256,256]{1,0:T(8,128)(2,1)S(1)}, bf16[256,256]{1,0:T(8,128)(2,1)}, u32[]{:S(2)}) copy-start(bf16[256,256]{1,0:T(8,128)(2,1)} %param.13) | copy-start | bytes 393220
  127.6 61.3 %reduce-scatter.3.cloned.1.call-start = ((), (), s32[]{:S(2)}) async-start(), calls=%async_computation.5 | async-start | bytes 1310720 | tf_op jit(solution)/shard_map/reduce_scatter | solution.py:53
  132.9 2.8 %copy-start.1 = (pred[256,2048]{0,1:T(8,128)(4,1)S(1)}, pred[256,2048]{0,1:T(8,128)(4,1)}, u32[]{:S(2)}) copy-start(pred[256,2048]{0,1:T(8,128)(4,1)} %iota_compare_fusion) | copy-start | bytes 1572868
  135.6 2.1 %copy-start.2 = (bf16[2048,256]{0,1:T(8,128)(2,1)S(1)}, bf16[2048,256]{0,1:T(8,128)(2,1)}, u32[]{:S(2)}) copy-start(bf16[2048,256]{0,1:T(8,128)(2,1)} %copy.44) | copy-start | bytes 3145732
  137.7 2.1 %copy-start.7 = (f32[2]{0:T(128)S(1)}, f32[2]{0:T(128)}, u32[]{:S(2)}) copy-start(f32[2]{0:T(128)} %param.16) | copy-start | bytes 28
  137.8 2.3 %copy-start.8 = (f32[128]{0:T(128)S(1)}, f32[128]{0:T(128)}, u32[]{:S(2)}) copy-start(f32[128]{0:T(128)} %param.17) | copy-start | bytes 1540
  139.9 26.7 %copy-start.6 = (f32[192,2]{0,1:T(2,128)S(1)}, f32[192,2]{0,1:T(2,128)}, u32[]{:S(2)}) copy-start(f32[192,2]{0,1:T(2,128)} %param.22) | copy-start | bytes 4612
  161.1 22.6 %all-to-all-start.1 = ((bf16[8,80,512]{2,1,0:T(8,128)(2,1)}), bf16[8,80,512]{2,1,0:T(8,128)(2,1)S(1)}, u32[]{:S(2)}, u32[]{:S(2)}) async-start(bf16[8,80,512]{2,1,0:T(8,128)(2,1)} %bitcast.85), calls=%async_computation.3 | async-start | bytes 1310720 | tf_op jit(solution)/shard_map/all_to_all | solution.py:102
Sparse Core Ops, SparseCore 0:
  27.3 81.9 all-gather.1
Sparse Core Ops, SparseCore 1:
  127.7 33.4 reduce-scatter.4
  164.1 24.7 reduce-scatter.2
